TPU v7x, 128 devices: a whole 4x4x4 slice. The times are simulated.
128 devices in a mesh: ep: 64 (over z, y, x), tp: 2 (over core).
Axes of the slice: x: 4, y: 4, z: 4, core: 2. Of those that a mesh axis runs over, the one named last changes fastest.
Arguments:
- tokens: bfloat16 [4096, 2048], P('ep', 'tp'), may hold values from -6 to 6
- sequence_state_real: float32 [4096, 128, 64], P('ep', 'tp'), may hold values from -4 to 4
- sequence_state_imaginary: float32 [4096, 128, 64], P('ep', 'tp'), may hold values from -4 to 4
- mixer_norm_gain: float32 [2048], replicated, may hold values from 0.1 to 1.9
- expert_norm_gain: float32 [2048], replicated, may hold values from 0.1 to 1.9
- rate: float32 [128, 64], P('tp'), may hold values from 0.1 to 4
- freq: float32 [128, 64], P('tp'), may hold values from -3 to 3
- log_group_step: float32 [128], P('tp'), may hold values from -3 to 0
- input_map_real: float32 [128, 64, 16], P('tp'), may hold values from -1 to 1
- input_map_imaginary: float32 [128, 64, 16], P('tp'), may hold values from -1 to 1
- output_map_real: float32 [128, 16, 64], P('tp'), may hold values from -0.75 to 0.75
- output_map_imaginary: float32 [128, 16, 64], P('tp'), may hold values from -0.75 to 0.75
- skip: float32 [2048], P('tp'), may hold values from -4 to 4
- mixer_value_weight: bfloat16 [2048, 2048], P('tp'), may hold values from -0.125 to 0.125
- mixer_gate_weight: bfloat16 [2048, 2048], P('tp'), may hold values from -0.125 to 0.125
- group_router_weight: bfloat16 [2048, 4], replicated, may hold values from -0.125 to 0.125
- expert_router_weight: bfloat16 [2048, 64], replicated, may hold values from -0.125 to 0.125
- dense_blend_weight: float32 [2048], replicated, may hold values from -0.125 to 0.125
- routes: int32 [4096, 2], P('ep'), may hold values from 0 to 63, all different within a row; in each aligned block of 64 rows (0 to 63, 64 to 127, ...) at most 4 rows name the same one
- expert_gate_weight: bfloat16 [64, 2048, 1024], P('ep', None, 'tp'), may hold values from -0.125 to 0.125
- expert_up_weight: bfloat16 [64, 2048, 1024], P('ep', None, 'tp'), may hold values from -0.125 to 0.125
- expert_down_weight: bfloat16 [64, 1024, 2048], P('ep', 'tp'), may hold values from -0.1875 to 0.1875
- shared_gate_weight: bfloat16 [2048, 2048], P('tp', 'ep'), may hold values from -0.125 to 0.125
- shared_up_weight: bfloat16 [2048, 2048], P('tp', 'ep'), may hold values from -0.125 to 0.125
- shared_down_weight: bfloat16 [2048, 2048], P(None, 'tp'), may hold values from -0.125 to 0.125
Outputs:
- result: bfloat16 [4096, 2048], P('ep', 'tp')
- next_re: float32 [4096, 128, 64], P('ep', 'tp')
- next_im: float32 [4096, 128, 64], P('ep', 'tp')
Inputs may be any that keep to these rules, and one draw needn't show every extreme that they name: `routes`: each row names 2 different experts. Among the rows of one device no expert is named more than 4 times, and in every draw some expert is named exactly 4 times by some device's rows.
All inputs are finite; a program needn't handle non-finite values.
Results may differ from a plain program's by a relative error of at most 0.017.
Values may be sent and summed in bfloat16 or wider, within the bound.
A program may use at most 128 MiB of HBM per device.

v0:
```python
import jax
import jax.numpy as jnp
from jax import lax
from jax.sharding import PartitionSpec as P

NG = 4
EPS = 1e-06


def total_of_pieces(x, axis):
    blocks = lax.all_gather(x, axis)
    return blocks.sum(axis=0)


def in_blocks(x, dim, size):
    lengths = x.shape
    blocks = x.reshape(*lengths[:dim], size, lengths[dim] // size, *lengths[dim + 1 :])
    return jnp.moveaxis(blocks, dim, 0)


def sent_and_summed(x, axis, dim):
    blocks = in_blocks(x, dim, lax.axis_size(axis))
    arrived = lax.all_to_all(blocks, axis, split_axis=0, concat_axis=0, tiled=True)
    return arrived.astype(jnp.float32).sum(axis=0)


def sent_to_all(x, axis):
    size = lax.axis_size(axis)
    return lax.all_to_all(jnp.broadcast_to(x[None], (size, *x.shape)), axis, 0, 0, tiled=True)


def over_copies(x, axis):
    return sent_to_all(x, axis).sum(axis=0)


def in_one(arrays, axis):
    ends = [0]
    for a in arrays:
        ends.append(ends[-1] + a.size)
    so_far = over_copies(jnp.concatenate([a.ravel() for a in arrays]), axis)
    return tuple((so_far[b:e].reshape(a.shape) for a, b, e in zip(arrays, ends, ends[1:])))


def joined_along(blocks, dim):
    lengths = list(blocks.shape[1:])
    lengths[dim] *= blocks.shape[0]
    return jnp.moveaxis(blocks, 0, dim).reshape(lengths)


def collect(x, axis, dim):
    return joined_along(sent_to_all(x, axis), dim)


def taken_together(x, axis):
    return sent_to_all(x, axis).astype(jnp.float32).sum(axis=0)


def state_factors(rate, freq, log_group_step, input_map_real, input_map_imaginary):
    step_size = jnp.exp(log_group_step)[:, None]
    magnitude = jnp.exp(-rate * step_size)
    abar_re = magnitude * jnp.cos(freq * step_size)
    abar_im = magnitude * jnp.sin(freq * step_size)
    denom = rate * rate + freq * freq
    shift_re = abar_re - 1.0
    fac_re = (abar_im * freq - shift_re * rate) / denom
    fac_im = -(abar_im * rate + shift_re * freq) / denom
    bbar_re = fac_re[:, :, None] * input_map_real - fac_im[:, :, None] * input_map_imaginary
    bbar_im = fac_re[:, :, None] * input_map_imaginary + fac_im[:, :, None] * input_map_real
    return (abar_re, abar_im, bbar_re, bbar_im)


def state_step(
    normed,
    sequence_state_real,
    sequence_state_imaginary,
    factors,
    output_map_real,
    output_map_imaginary,
    skip,
):
    abar_re, abar_im, bbar_re, bbar_im = factors
    groups = abar_re.shape[0]
    inputs = normed.astype(jnp.float32)
    grouped = inputs.reshape(inputs.shape[0], groups, -1)
    drive_re = jnp.einsum("tgc,gpc->tgp", grouped, bbar_re)
    drive_im = jnp.einsum("tgc,gpc->tgp", grouped, bbar_im)
    fresh_real = abar_re * sequence_state_real - abar_im * sequence_state_imaginary + drive_re
    fresh_imaginary = abar_re * sequence_state_imaginary + abar_im * sequence_state_real + drive_im
    state_readout = jnp.einsum("dor,zdr->zdo", output_map_real, fresh_real)
    state_readout = state_readout - jnp.einsum(
        "dor,zdr->zdo", output_map_imaginary, fresh_imaginary
    )
    mixed = state_readout.reshape(inputs.shape) + skip * inputs
    return (mixed, fresh_real, fresh_imaginary)


def pair_product(left, first_map, second_map):
    first = jnp.dot(left, first_map, preferred_element_type=jnp.float32)
    second = jnp.dot(left, second_map, preferred_element_type=jnp.float32)
    return jnp.concatenate([first, second], axis=1)


def shards(
    tokens,
    sequence_state_real,
    sequence_state_imaginary,
    mixer_norm_gain,
    expert_norm_gain,
    rate,
    freq,
    log_group_step,
    input_map_real,
    input_map_imaginary,
    output_map_real,
    output_map_imaginary,
    skip,
    mixer_value_weight,
    mixer_gate_weight,
    group_router_weight,
    expert_router_weight,
    dense_blend_weight,
    routes,
    expert_gate_weight,
    expert_up_weight,
    expert_down_weight,
    shared_gate_weight,
    shared_up_weight,
    shared_down_weight,
):
    seq_rows, half_width = tokens.shape
    width = 2 * half_width
    column_start = lax.axis_index("tp") * half_width

    def own_rows(values):
        return lax.dynamic_slice_in_dim(values, column_start, half_width, 0)

    float_tokens = tokens.astype(jnp.float32)
    square_sum = total_of_pieces(jnp.sum(float_tokens * float_tokens, axis=1), "tp")
    first_scale = lax.rsqrt(square_sum / width + EPS)[:, None]
    normed = (float_tokens * first_scale * own_rows(mixer_norm_gain)).astype(jnp.bfloat16)
    factors = state_factors(rate, freq, log_group_step, input_map_real, input_map_imaginary)
    mixed, next_re, next_im = state_step(
        normed,
        sequence_state_real,
        sequence_state_imaginary,
        factors,
        output_map_real,
        output_map_imaginary,
        skip,
    )
    activated = jax.nn.gelu(mixed).astype(jnp.bfloat16)
    value_part = jnp.dot(activated, mixer_value_weight, preferred_element_type=jnp.float32)
    gate_part = jnp.dot(activated, mixer_gate_weight, preferred_element_type=jnp.float32)
    stacked = jnp.stack([value_part, gate_part], axis=1)
    mix_sum = sent_and_summed(stacked.astype(jnp.bfloat16), "tp", 2)
    mix_half = (mix_sum[:, 0] * jax.nn.sigmoid(mix_sum[:, 1])).astype(jnp.bfloat16)
    hidden = (float_tokens + mix_half.astype(jnp.float32)).astype(jnp.bfloat16)
    hidden_f32 = hidden.astype(jnp.float32)
    scaled = hidden_f32 * own_rows(expert_norm_gain)
    router_map = jnp.concatenate(
        [own_rows(group_router_weight), own_rows(expert_router_weight)], axis=1
    ).astype(jnp.float32)
    blend_map = own_rows(dense_blend_weight)
    hidden_squares = jnp.sum(hidden_f32 * hidden_f32, axis=1)
    total_squares = total_of_pieces(hidden_squares, "tp")
    inverse = lax.rsqrt(total_squares / width + EPS)[:, None]
    normal_rows = scaled * inverse
    raw_part = jnp.dot(normal_rows, router_map)
    blend_part = jnp.dot(normal_rows, blend_map)
    logits, blend_logit = in_one((raw_part, blend_part), "tp")
    hnorm = (scaled * inverse).astype(jnp.bfloat16)
    experts = expert_router_weight.shape[1]
    top_count = routes.shape[1]
    per_group = experts // NG
    group_prob = jax.nn.softmax(logits[:, :NG], axis=-1)
    expert_logits = logits[:, NG:]
    expert_hits = routes[:, :, None] == jnp.arange(experts, dtype=jnp.int32)[None, None, :]
    chosen = jnp.sum(jnp.where(expert_hits, expert_logits[:, None, :], 0.0), axis=2)
    group_hits = (routes // per_group)[:, :, None] == jnp.arange(NG, dtype=jnp.int32)[None, None, :]
    group_sel = jnp.sum(jnp.where(group_hits, group_prob[:, None, :], 0.0), axis=2)
    weights = jax.nn.softmax(chosen, axis=1) * group_sel
    full_rows = collect(hnorm, "tp", 1)
    capacity = max(2, 2 * seq_rows * top_count // experts)
    flat_routes = routes.reshape(-1)
    matches = (flat_routes[:, None] == jnp.arange(experts, dtype=jnp.int32)[None, :]).astype(
        jnp.int32
    )
    slot_rank = jnp.sum(jnp.cumsum(matches, axis=0) * matches, axis=1) - 1
    slot_target = flat_routes * capacity + slot_rank
    dispatch = slot_target[None, :] == jnp.arange(experts * capacity, dtype=jnp.int32)[:, None]
    dispatch_rows = jnp.sum(
        dispatch.reshape(experts * capacity, seq_rows, top_count).astype(jnp.float32), axis=2
    )
    outgoing = jnp.dot(
        dispatch_rows.astype(jnp.bfloat16), full_rows, preferred_element_type=jnp.float32
    )
    outgoing = outgoing.astype(jnp.bfloat16).reshape(experts, capacity, width)
    received = lax.all_to_all(outgoing, "ep", split_axis=0, concat_axis=0, tiled=True)
    sources = received.shape[0]
    items = received.shape[1]
    token_rows = received.reshape(sources * items, width)
    gate_e = jnp.dot(token_rows, expert_gate_weight[0], preferred_element_type=jnp.float32)
    expert_up_rows = jnp.dot(token_rows, expert_up_weight[0], preferred_element_type=jnp.float32)
    inner = (jax.nn.silu(gate_e) * expert_up_rows).astype(jnp.bfloat16)
    part_out = jnp.dot(inner, expert_down_weight[0], preferred_element_type=jnp.float32)
    total = taken_together(part_out.astype(jnp.bfloat16), "tp").astype(jnp.float32)
    total = lax.dynamic_slice_in_dim(total, column_start, half_width, 1)
    finished = total.astype(jnp.bfloat16).reshape(sources, items, half_width)
    returned = lax.all_to_all(finished, "ep", split_axis=0, concat_axis=0, tiled=True)
    returned_flat = returned.reshape(experts * capacity, half_width)
    picked = returned_flat[slot_target].reshape(seq_rows, top_count, half_width).astype(jnp.float32)
    routed = jnp.sum(weights[:, :, None] * picked, axis=1)
    partial_dense = pair_product(
        lax.all_gather(hnorm, "ep", axis=0, tiled=True), shared_gate_weight, shared_up_weight
    )
    dense_sum = taken_together(partial_dense.astype(jnp.bfloat16), "tp").astype(jnp.float32)
    dense_cols = shared_gate_weight.shape[1]
    inner_cols = (jax.nn.silu(dense_sum[:, :dense_cols]) * dense_sum[:, dense_cols:]).astype(
        jnp.bfloat16
    )
    dense_inner = lax.all_to_all(inner_cols, "ep", split_axis=0, concat_axis=1, tiled=True)
    dense_out = jnp.dot(dense_inner, shared_down_weight, preferred_element_type=jnp.float32)
    result = hidden_f32 + routed + jax.nn.sigmoid(blend_logit)[:, None] * dense_out
    return (result.astype(jnp.bfloat16), next_re, next_im)


def solution(mesh):
    placed = (
        P("ep", "tp"),
        P("ep", "tp", None),
        P("ep", "tp", None),
        P(),
        P(),
        P("tp", None),
        P("tp", None),
        P("tp"),
        P("tp", None, None),
        P("tp", None, None),
        P("tp", None, None),
        P("tp", None, None),
        P("tp"),
        P("tp", None),
        P("tp", None),
        P(),
        P(),
        P(),
        P("ep", None),
        P("ep", None, "tp"),
        P("ep", None, "tp"),
        P("ep", "tp", None),
        P("tp", "ep"),
        P("tp", "ep"),
        P(None, "tp"),
    )
    return jax.shard_map(
        shards,
        mesh=mesh,
        in_specs=placed,
        out_specs=(P("ep", "tp"), P("ep", "tp", None), P("ep", "tp", None)),
        check_vma=False,
    )
```

profile of v0, /device:TPU:0, one launch (start us, length us, event | category | flops | bytes accessed | tf_op | source)
XLA Modules:
  0.0 192.3 jit_solution(11711179658692557491)
XLA Ops:
  7.2 3.5 %copy.204 = f32[64,64,64]{0,2,1:T(8,128)} copy(f32[64,64,64]{2,1,0:T(8,128)} %param.27) | data formatting | bytes 2097152 | tf_op args[2]
  10.7 3.4 %copy.203 = f32[64,64,64]{0,2,1:T(8,128)} copy(f32[64,64,64]{2,1,0:T(8,128)} %param.26) | data formatting | bytes 2097152 | tf_op args[1]
  14.3 0.6 dynamic-slice
  15.8 2.4 %all-reduce = f32[128]{0:T(128)S(1)} all-reduce(f32[128]{0:T(128)S(1)} %dynamic-update-slice), channel_id=2, replica_groups=mesh['ep'=64,'tp'=2] {'tp'}, use_global_device_ids=true, to_apply=%add | all-reduce | flops 128 | bytes 1024
  18.4 0.8 fusion.29
  19.1 1.1 copy.205
  20.2 1.0 fusion.65
  21.3 4.0 %bitcast_add_fusion.1 = f32[64,64,64]{0,2,1:T(8,128)S(1)} fusion(f32[64,64,64]{0,2,1:T(8,128)} %copy.204, f32[64,64,64]{0,2,1:T(8,128)} %copy.203, bf16[64,64,16]{0,2,1:T(8,128)(2,1)S(1)} %bitcast.73, f32[64,64]{1,0:T(8,128)S(1)} %get-tuple-element.30, f32[64,64]{1,0:T(8,128)S(1)} %get-tuple-element.31, f32[64,64,16]{1,2,0:T(8,128)S(1)} %copy-done.8, ...), kind=kOutput, calls=%fused_computation.14 | convolution fusion | flops 9633792 | bytes 3866624 | tf_op jit(solution)/shard_map/tgc,gpc->tgp/dot_general | solution.py:85
  25.3 2.4 %bitcast_add_fusion = f32[64,64,64]{0,2,1:T(8,128)S(1)} fusion(f32[64,64,64]{0,2,1:T(8,128)S(1)} %copy-done.6, f32[64,64,64]{0,2,1:T(8,128)S(1)} %copy-done.5, bf16[64,64,16]{0,2,1:T(8,128)(2,1)S(1)} %bitcast.74, f32[64,64]{1,0:T(8,128)S(1)} %get-tuple-element.30, f32[64,64]{1,0:T(8,128)S(1)} %get-tuple-element.31, f32[64,64,16]{1,2,0:T(8,128)S(1)} %copy-done.9, ...), kind=kOutput, calls=%fused_computation.13 | convolution fusion | flops 9633792 | bytes 3866624 | tf_op jit(solution)/shard_map/tgc,gpc->tgp/dot_general | solution.py:86
  28.2 1.0 copy-done.10
  29.2 0.4 convolution_subtract_fusion
  29.9 3.1 %convolution_convert_fusion.4 = bf16[64,2048]{1,0:T(8,128)(2,1)S(1)} fusion(bf16[1024,2048]{1,0:T(8,128)(2,1)} %param.39, f32[64,1024]{1,0:T(8,128)S(1)} %copy.210, f32[1024]{0:T(1024)S(1)} %copy-done.17, f32[1024]{0:T(1024)S(1)} %dynamic_slice.18, f32[64]{0:T(128)S(1)} %add_rsqrt_fusion.1, bf16[64,1024]{1,0:T(8,128)(2,1)S(1)} %copy-done.7), kind=kOutput, calls=%fused_computation.6 | convolution fusion | flops 269615104 | bytes 4858112 | tf_op jit(solution)/shard_map/dot_general | solution.py:153
  33.3 3.1 %convolution_convert_fusion.5 = bf16[64,2048]{1,0:T(8,128)(2,1)S(1)} fusion(bf16[1024,2048]{1,0:T(8,128)(2,1)} %param.38, f32[64,1024]{1,0:T(8,128)S(1)} %copy.210, f32[1024]{0:T(1024)S(1)} %copy-done.17, f32[1024]{0:T(1024)S(1)} %dynamic_slice.18, f32[64]{0:T(128)S(1)} %add_rsqrt_fusion.1, bf16[64,1024]{1,0:T(8,128)(2,1)S(1)} %copy-done.7), kind=kOutput, calls=%fused_computation.7 | convolution fusion | flops 269615104 | bytes 4858112 | tf_op jit(solution)/shard_map/dot_general | solution.py:152
  36.8 4.3 %all_to_all.57 = bf16[2,64,2,1024]{3,1,2,0:T(8,128)(2,1)S(1)} all-to-all(bf16[2,64,2,1024]{3,1,2,0:T(8,128)(2,1)S(1)} %maximum_bitcast_fusion), channel_id=1, replica_groups=mesh['ep'=64,'tp'=2] {'tp'}, dimensions={0} | all-to-all | bytes 1048576 | tf_op jit(solution)/shard_map/all_to_all | solution.py:23
  41.6 2.4 %all-reduce.1 = f32[128]{0:T(128)S(1)} all-reduce(f32[128]{0:T(128)S(1)} %dynamic-update-slice.1), channel_id=3, replica_groups=mesh['ep'=64,'tp'=2] {'tp'}, use_global_device_ids=true, to_apply=%add.1 | all-reduce | flops 128 | bytes 1024
  44.2 0.7 fusion.40
  45.0 1.6 broadcast_in_dim.33
  46.6 3.4 %all-to-all-start.2 = ((bf16[2,64,1024]{2,1,0:T(8,128)(2,1)}), bf16[2,64,1024]{2,1,0:T(8,128)(2,1)S(1)}, u32[]{:S(2)}, u32[]{:S(2)}) async-start(bf16[2,64,1024]{2,1,0:T(8,128)(2,1)} %broadcast_in_dim.33), calls=%async_computation.2 | async-start | bytes 524288 | tf_op jit(solution)/shard_map/all_to_all | solution.py:29
  50.7 0.9 all-to-all-done.2
  51.6 0.6 broadcast_in_dim.24
  52.2 3.9 %all-to-all-start.1 = ((f32[2,1,4416]{2,1,0:T(1,128)}), f32[2,1,4416]{2,1,0:T(1,128)}, u32[]{:S(2)}, u32[]{:S(2)}) async-start(f32[2,1,4416]{2,1,0:T(1,128)} %broadcast_in_dim.24), calls=%async_computation.1 | async-start | bytes 71680 | tf_op jit(solution)/shard_map/all_to_all | solution.py:29
  57.1 0.7 add_select_fusion
  57.9 0.4 convolution_convert_fusion.3
  58.4 1.2 reshape.198
  59.6 11.7 %all-to-all-start.3 = ((bf16[64,4,2048]{2,1,0:T(4,128)(2,1)}), bf16[64,4,2048]{2,1,0:T(4,128)(2,1)S(1)}, u32[]{:S(2)}, u32[]{:S(2)}) async-start(bf16[64,4,2048]{2,1,0:T(4,128)(2,1)} %reshape.198), calls=%async_computation.3 | async-start | bytes 2097152 | tf_op jit(solution)/shard_map/all_to_all | solution.py:198
  71.3 0.8 reduce_sum.140
  72.8 3.8 %copy.229 = f32[64,64,64]{2,1,0:T(8,128)} copy(f32[64,64,64]{0,2,1:T(8,128)} %copy-done.4) | data formatting | bytes 2097152
  76.5 3.8 %copy.230 = f32[64,64,64]{2,1,0:T(8,128)} copy(f32[64,64,64]{0,2,1:T(8,128)} %copy-done.3) | data formatting | bytes 2097152
  80.7 12.7 %all-to-all-done.3 = bf16[64,4,2048]{2,1,0:T(4,128)(2,1)S(1)} async-done(((bf16[64,4,2048]{2,1,0:T(4,128)(2,1)}), bf16[64,4,2048]{2,1,0:T(4,128)(2,1)S(1)}, u32[]{:S(2)}, u32[]{:S(2)}) %all-to-all-start.3) | async-done | bytes 1048608 | tf_op jit(solution)/shard_map/all_to_all | solution.py:198
  93.4 1.2 reshape.199
  94.6 3.4 %fusion.3 = f32[256,512]{1,0:T(8,128)} fusion(bf16[256,2048]{1,0:T(8,128)(2,1)} %reshape.199, bf16[1,2048,512]{2,1,0:T(8,128)(2,1)} %param.44), kind=kOutput, calls=%fused_computation.11 | convolution fusion | flops 536870912 | bytes 3670016 | tf_op jit(solution)/shard_map/dot_general | solution.py:202
  98.0 3.3 %convolution_convert_fusion.2 = bf16[256,2048]{1,0:T(8,128)(2,1)S(1)} fusion(bf16[1,512,2048]{2,1,0:T(8,128)(2,1)S(1)} %copy-done, bf16[256,2048]{1,0:T(8,128)(2,1)} %reshape.199, bf16[1,2048,512]{2,1,0:T(8,128)(2,1)} %param.45, f32[256,512]{1,0:T(8,128)} %fusion.3), kind=kOutput, calls=%fused_computation.4 | convolution fusion | flops 1075052544 | bytes 6815744 | tf_op jit(solution)/shard_map/dot_general | solution.py:205
  101.6 5.4 %all_to_all.55 = bf16[2,256,2048]{2,1,0:T(8,128)(2,1)S(1)} all-to-all(bf16[2,256,2048]{2,1,0:T(8,128)(2,1)S(1)} %broadcast_in_dim.34), channel_id=1, replica_groups=mesh['ep'=64,'tp'=2] {'tp'}, dimensions={0} | all-to-all | bytes 4194304 | tf_op jit(solution)/shard_map/all_to_all | solution.py:29
  107.0 0.4 convert_reduce_fusion
  107.5 1.0 reshape.200
  108.5 21.7 %all-gather.4.cloned.1.call-done = bf16[4096,1024]{1,0:T(8,128)(2,1)} async-done(((bf16[64,1024]{1,0:T(8,128)(2,1)}), bf16[4096,1024]{1,0:T(8,128)(2,1)}) %all-gather.4.cloned.1.call-update) | async-done | bytes 8388624 | tf_op jit(solution)/shard_map/all_gather | solution.py:214
  130.2 6.1 %convolution_convert_fusion = bf16[4096,32]{0,1:T(8,128)(2,1)S(1)} fusion(bf16[4096,1024]{1,0:T(8,128)(2,1)} %all-gather.4.cloned.1.call-done, bf16[1024,32]{0,1:T(8,128)(2,1)S(1)} %copy-done.14), kind=kOutput, calls=%fused_computation.1 | convolution fusion | flops 268566528 | bytes 8716288 | tf_op jit(solution)/shard_map/dot_general | solution.py:99
  136.3 2.5 %convolution_convert_fusion.1 = bf16[4096,32]{0,1:T(8,128)(2,1)S(1)} fusion(bf16[4096,1024]{1,0:T(8,128)(2,1)S(1)} %copy-done.2, bf16[1024,32]{0,1:T(8,128)(2,1)S(1)} %copy-done.15), kind=kOutput, calls=%fused_computation.2 | convolution fusion | flops 268566528 | bytes 8716288 | tf_op jit(solution)/shard_map/dot_general | solution.py:98
  139.0 4.6 %all_to_all.56 = bf16[2,4096,64]{1,2,0:T(8,128)(2,1)S(1)} all-to-all(bf16[2,4096,64]{1,2,0:T(8,128)(2,1)S(1)} %broadcast_in_dim.35), channel_id=1, replica_groups=mesh['ep'=64,'tp'=2] {'tp'}, dimensions={0} | all-to-all | bytes 2097152 | tf_op jit(solution)/shard_map/all_to_all | solution.py:29
  143.6 8.6 %all-to-all-start.5 = ((bf16[64,4,1024]{2,1,0:T(4,128)(2,1)}), bf16[64,4,1024]{2,1,0:T(4,128)(2,1)S(1)}, u32[]{:S(2)}, u32[]{:S(2)}) async-start(bf16[64,4,1024]{2,1,0:T(4,128)(2,1)} %reshape.200), calls=%async_computation.5 | async-start | bytes 1048576 | tf_op jit(solution)/shard_map/all_to_all | solution.py:209
  152.5 0.5 all_to_all.43
  153.4 1.0 reshape.228
  154.4 11.4 %all-to-all-done.5 = bf16[64,4,1024]{2,1,0:T(4,128)(2,1)S(1)} async-done(((bf16[64,4,1024]{2,1,0:T(4,128)(2,1)}), bf16[64,4,1024]{2,1,0:T(4,128)(2,1)S(1)}, u32[]{:S(2)}, u32[]{:S(2)}) %all-to-all-start.5) | async-done | bytes 524320 | tf_op jit(solution)/shard_map/all_to_all | solution.py:209
  165.9 5.0 %all-to-all-start.7 = ((bf16[64,2,1024]{2,1,0:T(2,128)(2,1)}), bf16[64,2,1024]{2,1,0:T(2,128)(2,1)S(1)}, u32[]{:S(2)}, u32[]{:S(2)}) async-start(bf16[64,2,1024]{2,1,0:T(2,128)(2,1)} %reshape.228), calls=%async_computation.7 | async-start | bytes 524288 | tf_op jit(solution)/shard_map/all_to_all | solution.py:221
  171.0 0.9 gather_fusion
  172.2 0.7 multiply_reduce_fusion
  172.9 8.3 %all-to-all-done.7 = bf16[64,2,1024]{2,1,0:T(2,128)(2,1)S(1)} async-done(((bf16[64,2,1024]{2,1,0:T(2,128)(2,1)}), bf16[64,2,1024]{2,1,0:T(2,128)(2,1)S(1)}, u32[]{:S(2)}, u32[]{:S(2)}) %all-to-all-start.7) | async-done | bytes 262176 | tf_op jit(solution)/shard_map/all_to_all | solution.py:221
  181.6 3.9 %fusion.12 = bf16[64,1024]{1,0:T(8,128)(2,1)} fusion(bf16[64,2048]{0,1:T(8,128)(2,1)S(1)} %bitcast.77, bf16[2048,1024]{1,0:T(8,128)(2,1)} %param.49, f32[64,1024]{1,0:T(8,128)S(1)} %multiply_reduce_fusion, bf16[64,1024]{1,0:T(8,128)(2,1)S(1)} %get-tuple-element.28, f32[64]{0:T(128)S(1)} %fusion.73), kind=kOutput, calls=%fused_computation.21 | convolution fusion | flops 268763136 | bytes 4980992 | tf_op jit(solution)/shard_map/dot_general | solution.py:222
  (120 shorter events, 7.1 us)
Async XLA Ops:
  7.2 90.8 %copy-start = (bf16[1,512,2048]{2,1,0:T(8,128)(2,1)S(1)}, bf16[1,512,2048]{2,1,0:T(8,128)(2,1)}, u32[]{:S(2)}) copy-start(bf16[1,512,2048]{2,1,0:T(8,128)(2,1)} %param.46) | copy-start | bytes 6291460
  7.2 123.0 %all-gather.4.cloned.1.call-start = ((), (), s32[]{:S(2)}) async-start(), calls=%async_computation.8 | async-start | bytes 8519680 | tf_op jit(solution)/shard_map/all_gather | solution.py:214
  10.7 3.5 %copy-start.7 = (bf16[64,1024]{1,0:T(8,128)(2,1)S(1)}, bf16[64,1024]{1,0:T(8,128)(2,1)}, u32[]{:S(2)}) copy-start(bf16[64,1024]{1,0:T(8,128)(2,1)} %param.25) | copy-start | bytes 393220
  10.7 3.6 %copy-start.23 = (u32[128]{0:T(128)S(1)}, u32[128]{0:T(128)}, u32[]{:S(2)}) copy-start(u32[128]{0:T(128)} %constant.69) | copy-start | bytes 1540
  10.7 7.6 %copy-start.20 = (f32[2048]{0:T(1024)S(1)}, f32[2048]{0:T(1024)}, u32[]{:S(2)}) copy-start(f32[2048]{0:T(1024)} %param.28) | copy-start | bytes 24580
  10.7 9.5 %copy-start.22 = (f32[64]{0:T(128)S(1)}, f32[64]{0:T(128)}, u32[]{:S(2)}) copy-start(f32[64]{0:T(128)} %param.32) | copy-start | bytes 772
  10.7 10.5 %copy-start.8 = (f32[64,64,16]{1,2,0:T(8,128)S(1)}, f32[64,64,16]{1,2,0:T(8,128)}, u32[]{:S(2)}) copy-start(f32[64,64,16]{1,2,0:T(8,128)} %param.34) | copy-start | bytes 786436
  10.7 10.5 %copy-start.9 = (f32[64,64,16]{1,2,0:T(8,128)S(1)}, f32[64,64,16]{1,2,0:T(8,128)}, u32[]{:S(2)}) copy-start(f32[64,64,16]{1,2,0:T(8,128)} %param.33) | copy-start | bytes 786436
  21.2 4.0 %copy-start.5 = (f32[64,64,64]{0,2,1:T(8,128)S(1)}, f32[64,64,64]{0,2,1:T(8,128)}, u32[]{:S(2)}) copy-start(f32[64,64,64]{0,2,1:T(8,128)} %copy.204) | copy-start | bytes 3145732
  21.2 4.0 %copy-start.6 = (f32[64,64,64]{0,2,1:T(8,128)S(1)}, f32[64,64,64]{0,2,1:T(8,128)}, u32[]{:S(2)}) copy-start(f32[64,64,64]{0,2,1:T(8,128)} %copy.203) | copy-start | bytes 3145732
  25.3 2.5 %copy-start.4 = (f32[64,64,64]{0,2,1:T(8,128)}, f32[64,64,64]{0,2,1:T(8,128)S(1)}, u32[]{:S(2)}) copy-start(f32[64,64,64]{0,2,1:T(8,128)S(1)} %bitcast_add_fusion.1) | copy-start | bytes 3145732
  25.3 2.5 %copy-start.11 = (f32[64,16,64]{2,1,0:T(8,128)S(1)}, f32[64,16,64]{2,1,0:T(8,128)}, u32[]{:S(2)}) copy-start(f32[64,16,64]{2,1,0:T(8,128)} %param.35) | copy-start | bytes 786436
  27.8 1.9 copy-start.3
  27.8 1.4 copy-start.10
  29.2 0.7 copy-start.17
  36.7 7.5 %copy-start.21 = (f32[2048]{0:T(1024)S(1)}, f32[2048]{0:T(1024)}, u32[]{:S(2)}) copy-start(f32[2048]{0:T(1024)} %param.29) | copy-start | bytes 24580
  36.8 13.3 %copy-start.19 = (bf16[2048,4]{0,1:T(4,128)(2,1)S(1)}, bf16[2048,4]{0,1:T(4,128)(2,1)}, u32[]{:S(2)}) copy-start(bf16[2048,4]{0,1:T(4,128)(2,1)} %param.40) | copy-start | bytes 49156
  36.8 13.3 %copy-start.16 = (bf16[2048,64]{0,1:T(8,128)(2,1)S(1)}, bf16[2048,64]{0,1:T(8,128)(2,1)}, u32[]{:S(2)}) copy-start(bf16[2048,64]{0,1:T(8,128)(2,1)} %param.41) | copy-start | bytes 786436
  41.1 9.4 %dynamic-slice-start = ((f32[2048]{0:T(1024)}, s32[]{:T(128)}), f32[1024]{0:T(1024)S(1)}, s32[]{:S(2)}) async-start(f32[2048]{0:T(1024)} %param.42, s32[]{:T(128)} %select_n.31), calls=%async_computation.9 | async-start | bytes 8704 | tf_op jit(solution)/shard_map/dynamic_slice | solution.py:135
  41.2 15.0 %copy-start.18 = (s32[64,2]{0,1:T(2,128)S(1)}, s32[64,2]{0,1:T(2,128)}, u32[]{:S(2)}) copy-start(s32[64,2]{0,1:T(2,128)} %param.43) | copy-start | bytes 1540
  46.6 5.0 %all-to-all-start.2 = ((bf16[2,64,1024]{2,1,0:T(8,128)(2,1)}), bf16[2,64,1024]{2,1,0:T(8,128)(2,1)S(1)}, u32[]{:S(2)}, u32[]{:S(2)}) async-start(bf16[2,64,1024]{2,1,0:T(8,128)(2,1)} %broadcast_in_dim.33), calls=%async_computation.2 | async-start | bytes 524288 | tf_op jit(solution)/shard_map/all_to_all | solution.py:29
  52.2 7.4 %all-to-all-start.1 = ((f32[2,1,4416]{2,1,0:T(1,128)}), f32[2,1,4416]{2,1,0:T(1,128)}, u32[]{:S(2)}, u32[]{:S(2)}) async-start(f32[2,1,4416]{2,1,0:T(1,128)} %broadcast_in_dim.24), calls=%async_computation.1 | async-start | bytes 71680 | tf_op jit(solution)/shard_map/all_to_all | solution.py:29
  59.6 33.8 %all-to-all-start.3 = ((bf16[64,4,2048]{2,1,0:T(4,128)(2,1)}), bf16[64,4,2048]{2,1,0:T(4,128)(2,1)S(1)}, u32[]{:S(2)}, u32[]{:S(2)}) async-start(bf16[64,4,2048]{2,1,0:T(4,128)(2,1)} %reshape.198), calls=%async_computation.3 | async-start | bytes 2097152 | tf_op jit(solution)/shard_map/all_to_all | solution.py:198
  76.5 3.8 %copy-start.13 = (s32[64,2]{1,0:T(8,128)S(1)}, s32[64,2]{1,0:T(8,128)}, u32[]{:S(2)}) copy-start(s32[64,2]{1,0:T(8,128)} %get-tuple-element.35) | copy-start | bytes 1540
  76.5 3.9 %copy-start.12 = (s32[64,2]{1,0:T(8,128)S(1)}, s32[64,2]{1,0:T(8,128)}, u32[]{:S(2)}) copy-start(s32[64,2]{1,0:T(8,128)} %get-tuple-element.33) | copy-start | bytes 1540
  107.0 23.2 %copy-start.14 = (bf16[1024,32]{0,1:T(8,128)(2,1)S(1)}, bf16[1024,32]{0,1:T(8,128)(2,1)}, u32[]{:S(2)}) copy-start(bf16[1024,32]{0,1:T(8,128)(2,1)} %param.48) | copy-start | bytes 196612
  108.5 27.8 %copy-start.15 = (bf16[1024,32]{0,1:T(8,128)(2,1)S(1)}, bf16[1024,32]{0,1:T(8,128)(2,1)}, u32[]{:S(2)}) copy-start(bf16[1024,32]{0,1:T(8,128)(2,1)} %param.47) | copy-start | bytes 196612
  130.2 6.1 %copy-start.2 = (bf16[4096,1024]{1,0:T(8,128)(2,1)S(1)}, bf16[4096,1024]{1,0:T(8,128)(2,1)}, u32[]{:S(2)}) copy-start(bf16[4096,1024]{1,0:T(8,128)(2,1)} %all-gather.4.cloned.1.call-done) | copy-start | bytes 25165828
  143.6 22.3 %all-to-all-start.5 = ((bf16[64,4,1024]{2,1,0:T(4,128)(2,1)}), bf16[64,4,1024]{2,1,0:T(4,128)(2,1)S(1)}, u32[]{:S(2)}, u32[]{:S(2)}) async-start(bf16[64,4,1024]{2,1,0:T(4,128)(2,1)} %reshape.200), calls=%async_computation.5 | async-start | bytes 1048576 | tf_op jit(solution)/shard_map/all_to_all | solution.py:209
  165.9 15.3 %all-to-all-start.7 = ((bf16[64,2,1024]{2,1,0:T(2,128)(2,1)}), bf16[64,2,1024]{2,1,0:T(2,128)(2,1)S(1)}, u32[]{:S(2)}, u32[]{:S(2)}) async-start(bf16[64,2,1024]{2,1,0:T(2,128)(2,1)} %reshape.228), calls=%async_computation.7 | async-start | bytes 524288 | tf_op jit(solution)/shard_map/all_to_all | solution.py:221
  181.6 3.9 %copy-start.1 = (bf16[1,512,2048]{2,1,0:T(8,128)(2,1)S(1)}, bf16[1,512,2048]{2,1,0:T(8,128)(2,1)}, u32[]{:S(2)}) copy-start(bf16[1,512,2048]{2,1,0:T(8,128)(2,1)} %param.46) | copy-start | bytes 6291460
Sparse Core Ops, SparseCore 0:
  45.1 85.0 all-gather.3
where the time goes:
time: 193 us; the launch traced here: 192 us
  waiting for transfers between devices  55 us (28%)
  matrix products  33.7 us (17%)
  starting transfers between devices  32.6 us (17%)
  local copies, waits for them, and re-layouts  29.5 us (15%)
  blocking collectives  19.2 us (10%)
  between operations  15.3 us (8%)
  other arithmetic  6.95 us (4%)
    all_gather x1, waiting for transfers between devices, shards(): lax.all_gather(hnorm, 'ep', axis=0, tiled=True)  21.7 us
    unnamed x61, local copies, waits for them, and re-layouts  18.2 us
    all_to_all x1, waiting for transfers between devices, shards(): lax.all_to_all(outgoing, 'ep', split_axis=0, concat_axis=0, tiled=True)  12.7 us
    all_to_all x1, starting transfers between devices, shards(): lax.all_to_all(outgoing, 'ep', split_axis=0, concat_axis=0, tiled=True)  11.7 us
    all_to_all x1, waiting for transfers between devices, shards(): lax.all_to_all(finished, 'ep', split_axis=0, concat_axis=0, tiled=True)  11.4 us
    all_to_all x2, blocking collectives, sent_to_all(): lax.all_to_all(jnp.broadcast_to(x[None], (size, *x.shape)), axis, 0, 0, t...  9.99 us
    all_to_all x1, starting transfers between devices, shards(): lax.all_to_all(finished, 'ep', split_axis=0, concat_axis=0, tiled=True)  8.6 us
    all_to_all x1, waiting for transfers between devices, shards(): lax.all_to_all(inner_cols, 'ep', split_axis=0, concat_axis=1, tiled=True)  8.32 us
  transfers between devices with their start and end apart: 6, of which 5 were waited for; matrix products, arithmetic and copies ran while one was open for 15% of the time, Pallas kernels for 0%

commit v1 on v0

--- a/solution.py
+++ b/solution.py
@@ -5,6 +5,11 @@
 
 NG = 4
 EPS = 1e-06
+
+
+def gather_over(block, axis, dim):
+    sent = jnp.stack([block] * lax.axis_size(axis))
+    return jnp.concatenate(lax.all_to_all(sent, axis, 0, 0), axis=dim)
 
 
 def total_of_pieces(x, axis):
@@ -210,9 +215,7 @@
     returned_flat = returned.reshape(experts * capacity, half_width)
     picked = returned_flat[slot_target].reshape(seq_rows, top_count, half_width).astype(jnp.float32)
     routed = jnp.sum(weights[:, :, None] * picked, axis=1)
-    partial_dense = pair_product(
-        lax.all_gather(hnorm, "ep", axis=0, tiled=True), shared_gate_weight, shared_up_weight
-    )
+    partial_dense = pair_product(gather_over(hnorm, "ep", 0), shared_gate_weight, shared_up_weight)
     dense_sum = taken_together(partial_dense.astype(jnp.bfloat16), "tp").astype(jnp.float32)
     dense_cols = shared_gate_weight.shape[1]
     inner_cols = (jax.nn.silu(dense_sum[:, :dense_cols]) * dense_sum[:, dense_cols:]).astype(

time: 193 us -> 293 us (1.52)
  waiting for transfers between devices: 55 us -> 146 us
  starting transfers between devices: 32.6 us -> 46.1 us
  between operations: 15.3 us -> 1.97 us
  matrix products: 33.7 us -> 37.9 us
  local copies, waits for them, and re-layouts: 29.5 us -> 33.4 us
    all_to_all x0 -> x1, waiting for transfers between devices: none -> 107 us  [gather_over(): return jnp.concatenate(lax.all_to_all(sent, axis, 0, 0), axis=dim)]
    all_gather x1 -> x0, waiting for transfers between devices: 21.7 us -> none  [shards(): lax.all_gather(hnorm, 'ep', axis=0, tiled=True)]
    all_to_all x1, starting transfers between devices: 8.6 us -> 16.9 us  [shards(): lax.all_to_all(finished, 'ep', split_axis=0, concat_axis=0, tiled=True)]
    all_to_all x0 -> x1, starting transfers between devices: none -> 5.93 us  [gather_over(): return jnp.concatenate(lax.all_to_all(sent, axis, 0, 0), axis=dim)]
    all_to_all x1, waiting for transfers between devices: 12.7 us -> 17.7 us  [shards(): lax.all_to_all(outgoing, 'ep', split_axis=0, concat_axis=0, tiled=True)]
    another operation x0 -> x1, local copies, waits for them, and re-layouts: none -> 4.28 us  [gather_over(): sent = jnp.stack([block] * lax.axis_size(axis))]
    dot_general x1, matrix products: 2.55 us -> 5.93 us  [pair_product(): first = jnp.dot(left, first_map, preferred_element_type=jnp.float32)]
    unnamed x61 -> x55, local copies, waits for them, and re-layouts: 18.2 us -> 17.3 us
  transfers between devices with their start and end apart: 6 -> 6, of which waited for: 5 -> 5; matrix products, arithmetic and copies ran while one was open for 15% -> 8% of each run, Pallas kernels for 0% -> 0%
where the time goes in v1:
time: 293 us; the launch traced here: 292 us
  waiting for transfers between devices  146 us (50%)
  starting transfers between devices  46.1 us (16%)
  matrix products  37.9 us (13%)
  local copies, waits for them, and re-layouts  33.4 us (11%)
  blocking collectives  19.9 us (7%)
  other arithmetic  6.54 us (2%)
    all_to_all x1, waiting for transfers between devices, gather_over(): return jnp.concatenate(lax.all_to_all(sent, axis, 0, 0), axis=dim)  107 us
    all_to_all x1, waiting for transfers between devices, shards(): lax.all_to_all(outgoing, 'ep', split_axis=0, concat_axis=0, tiled=True)  17.7 us
    unnamed x55, local copies, waits for them, and re-layouts  17.3 us
    all_to_all x1, starting transfers between devices, shards(): lax.all_to_all(finished, 'ep', split_axis=0, concat_axis=0, tiled=True)  16.9 us
    all_to_all x1, starting transfers between devices, shards(): lax.all_to_all(outgoing, 'ep', split_axis=0, concat_axis=0, tiled=True)  11.5 us
    all_to_all x1, waiting for transfers between devices, shards(): lax.all_to_all(finished, 'ep', split_axis=0, concat_axis=0, tiled=True)  11.4 us
    all_to_all x2, blocking collectives, sent_to_all(): lax.all_to_all(jnp.broadcast_to(x[None], (size, *x.shape)), axis, 0, 0, t...  10.9 us
    all_to_all x1, waiting for transfers between devices, shards(): lax.all_to_all(inner_cols, 'ep', split_axis=0, concat_axis=1, tiled=True)  8.32 us
  transfers between devices with their start and end apart: 6, of which 5 were waited for; matrix products, arithmetic and copies ran while one was open for 8% of the time, Pallas kernels for 0%

profile of v1, /device:TPU:0, one launch (start us, length us, event | category | flops | bytes accessed | tf_op | source)
XLA Modules:
  0.0 291.9 jit_solution(5431180281741382593)
XLA Ops:
  0.7 3.5 %copy.204 = f32[64,64,64]{0,2,1:T(8,128)} copy(f32[64,64,64]{2,1,0:T(8,128)} %param.27) | data formatting | bytes 2097152 | tf_op args[2]
  4.2 3.4 %copy.203 = f32[64,64,64]{0,2,1:T(8,128)} copy(f32[64,64,64]{2,1,0:T(8,128)} %param.26) | data formatting | bytes 2097152 | tf_op args[1]
  7.7 0.6 dynamic-slice
  9.2 2.4 all-reduce
  11.8 0.8 fusion.29
  12.5 1.1 copy.205
  13.6 1.0 fusion.65
  14.7 4.0 %bitcast_add_fusion.1 = f32[64,64,64]{0,2,1:T(8,128)S(1)} fusion(f32[64,64,64]{0,2,1:T(8,128)} %copy.204, f32[64,64,64]{0,2,1:T(8,128)} %copy.203, bf16[64,64,16]{0,2,1:T(8,128)(2,1)S(1)} %bitcast.74, f32[64,64]{1,0:T(8,128)S(1)} %get-tuple-element.30, f32[64,64]{1,0:T(8,128)S(1)} %get-tuple-element.31, f32[64,64,16]{1,2,0:T(8,128)S(1)} %copy-done.8, ...), kind=kOutput, calls=%fused_computation.14 | convolution fusion | flops 9633792 | bytes 3866624 | tf_op jit(solution)/shard_map/tgc,gpc->tgp/dot_general | solution.py:90
  18.7 2.4 bitcast_add_fusion
  21.6 1.0 copy-done.10
  23.3 3.1 %convolution_convert_fusion.4 = bf16[64,2048]{1,0:T(8,128)(2,1)S(1)} fusion(bf16[1024,2048]{1,0:T(8,128)(2,1)} %param.39, f32[64,1024]{1,0:T(8,128)S(1)} %copy.210, f32[1024]{0:T(1024)S(1)} %copy-done.14, f32[1024]{0:T(1024)S(1)} %dynamic_slice.18, f32[64]{0:T(128)S(1)} %add_rsqrt_fusion.1, bf16[64,1024]{1,0:T(8,128)(2,1)S(1)} %copy-done.7), kind=kOutput, calls=%fused_computation.6 | convolution fusion | flops 269615104 | bytes 4858112 | tf_op jit(solution)/shard_map/dot_general | solution.py:158
  26.7 3.1 %convolution_convert_fusion.5 = bf16[64,2048]{1,0:T(8,128)(2,1)S(1)} fusion(bf16[1024,2048]{1,0:T(8,128)(2,1)} %param.38, f32[64,1024]{1,0:T(8,128)S(1)} %copy.210, f32[1024]{0:T(1024)S(1)} %copy-done.14, f32[1024]{0:T(1024)S(1)} %dynamic_slice.18, f32[64]{0:T(128)S(1)} %add_rsqrt_fusion.1, bf16[64,1024]{1,0:T(8,128)(2,1)S(1)} %copy-done.7), kind=kOutput, calls=%fused_computation.7 | convolution fusion | flops 269615104 | bytes 4858112 | tf_op jit(solution)/shard_map/dot_general | solution.py:157
  30.2 4.2 %all_to_all.62 = bf16[2,64,2,1024]{3,1,2,0:T(8,128)(2,1)S(1)} all-to-all(bf16[2,64,2,1024]{3,1,2,0:T(8,128)(2,1)S(1)} %maximum_bitcast_fusion), channel_id=1, replica_groups=mesh['ep'=64,'tp'=2] {'tp'}, dimensions={0} | all-to-all | bytes 1048576 | tf_op jit(solution)/shard_map/all_to_all | solution.py:28
  34.9 2.4 all-reduce.1
  37.6 0.7 broadcast_in_dim.33
  38.3 3.4 %all-to-all-start.2 = ((bf16[2,64,1024]{2,1,0:T(8,128)(2,1)}), bf16[2,64,1024]{2,1,0:T(8,128)(2,1)S(1)}, u32[]{:S(2)}, u32[]{:S(2)}) async-start(bf16[2,64,1024]{2,1,0:T(8,128)(2,1)} %broadcast_in_dim.33), calls=%async_computation.2 | async-start | bytes 524288 | tf_op jit(solution)/shard_map/all_to_all | solution.py:34
  41.9 1.4 all-to-all-done.2
  43.3 0.7 copy.244
  45.1 1.4 convolution_convert_fusion.3
  46.5 1.2 reshape.203
  47.7 11.5 %all-to-all-start.3 = ((bf16[64,4,2048]{2,1,0:T(4,128)(2,1)}), bf16[64,4,2048]{2,1,0:T(4,128)(2,1)S(1)}, u32[]{:S(2)}, u32[]{:S(2)}) async-start(bf16[64,4,2048]{2,1,0:T(4,128)(2,1)} %reshape.203), calls=%async_computation.3 | async-start | bytes 2097152 | tf_op jit(solution)/shard_map/all_to_all | solution.py:203
  59.3 0.9 constant_dynamic-slice_fusion
  60.8 17.7 %all-to-all-done.3 = bf16[64,4,2048]{2,1,0:T(4,128)(2,1)S(1)} async-done(((bf16[64,4,2048]{2,1,0:T(4,128)(2,1)}), bf16[64,4,2048]{2,1,0:T(4,128)(2,1)S(1)}, u32[]{:S(2)}, u32[]{:S(2)}) %all-to-all-start.3) | async-done | bytes 1048608 | tf_op jit(solution)/shard_map/all_to_all | solution.py:203
  78.5 0.6 broadcast_in_dim.24
  79.1 3.3 %all-to-all-start.1 = ((f32[2,1,4416]{2,1,0:T(1,128)}), f32[2,1,4416]{2,1,0:T(1,128)S(1)}, u32[]{:S(2)}, u32[]{:S(2)}) async-start(f32[2,1,4416]{2,1,0:T(1,128)} %broadcast_in_dim.24), calls=%async_computation.1 | async-start | bytes 71680 | tf_op jit(solution)/shard_map/all_to_all | solution.py:34
  82.4 1.1 reshape.204
  83.5 3.4 %fusion.3 = f32[256,512]{1,0:T(8,128)} fusion(bf16[256,2048]{1,0:T(8,128)(2,1)} %reshape.204, bf16[1,2048,512]{2,1,0:T(8,128)(2,1)} %param.44), kind=kOutput, calls=%fused_computation.11 | convolution fusion | flops 536870912 | bytes 3670016 | tf_op jit(solution)/shard_map/dot_general | solution.py:207
  86.9 3.3 %convolution_convert_fusion.2 = bf16[256,2048]{1,0:T(8,128)(2,1)S(1)} fusion(bf16[1,512,2048]{2,1,0:T(8,128)(2,1)S(1)} %copy-done, bf16[256,2048]{1,0:T(8,128)(2,1)} %reshape.204, bf16[1,2048,512]{2,1,0:T(8,128)(2,1)} %param.45, f32[256,512]{1,0:T(8,128)} %fusion.3), kind=kOutput, calls=%fused_computation.4 | convolution fusion | flops 1075052544 | bytes 6815744 | tf_op jit(solution)/shard_map/dot_general | solution.py:210
  90.5 6.3 %all_to_all.60 = bf16[2,256,2048]{2,1,0:T(8,128)(2,1)} all-to-all(bf16[2,256,2048]{2,1,0:T(8,128)(2,1)S(1)} %broadcast_in_dim.34), channel_id=1, replica_groups=mesh['ep'=64,'tp'=2] {'tp'}, dimensions={0} | all-to-all | bytes 4194304 | tf_op jit(solution)/shard_map/all_to_all | solution.py:34
  96.8 4.3 %stack.11 = bf16[64,64,1024]{2,1,0:T(8,128)(2,1)} broadcast(bf16[64,1024]{1,0:T(8,128)(2,1)S(1)} %fusion.40), dimensions={1,2} | broadcast | bytes 8519680 | tf_op jit(solution)/shard_map/stack | solution.py:11
  101.1 5.9 %all-to-all-start.6 = ((bf16[64,64,1024]{2,1,0:T(8,128)(2,1)}), bf16[64,64,1024]{2,1,0:T(8,128)(2,1)}, u32[]{:S(2)}, u32[]{:S(2)}) async-start(bf16[64,64,1024]{2,1,0:T(8,128)(2,1)} %stack.11), calls=%async_computation.6 | async-start | bytes 16777216 | tf_op jit(solution)/shard_map/all_to_all | solution.py:12
  107.0 3.9 %copy.229 = f32[64,64,64]{2,1,0:T(8,128)} copy(f32[64,64,64]{0,2,1:T(8,128)} %copy-done.4) | data formatting | bytes 2097152
  110.9 2.7 copy.230
  114.7 2.0 convert_reduce_fusion
  116.8 1.0 reshape.205
  117.8 107.2 %all-to-all-done.6 = bf16[64,64,1024]{2,1,0:T(8,128)(2,1)} async-done(((bf16[64,64,1024]{2,1,0:T(8,128)(2,1)}), bf16[64,64,1024]{2,1,0:T(8,128)(2,1)}, u32[]{:S(2)}, u32[]{:S(2)}) %all-to-all-start.6) | async-done | bytes 8388640 | tf_op jit(solution)/shard_map/all_to_all | solution.py:12
  225.0 6.0 %convolution_convert_fusion = bf16[4096,32]{0,1:T(8,128)(2,1)S(1)} fusion(bf16[4096,1024]{1,0:T(8,128)(2,1)} %bitcast.16, bf16[1024,32]{0,1:T(8,128)(2,1)S(1)} %copy-done.12), kind=kOutput, calls=%fused_computation.1 | convolution fusion | flops 268566528 | bytes 8716288 | tf_op jit(solution)/shard_map/dot_general | solution.py:104
  231.0 5.9 %convolution_convert_fusion.1 = bf16[4096,32]{0,1:T(8,128)(2,1)S(1)} fusion(bf16[4096,1024]{1,0:T(8,128)(2,1)} %bitcast.16, bf16[1024,32]{0,1:T(8,128)(2,1)S(1)} %copy-done.13), kind=kOutput, calls=%fused_computation.2 | convolution fusion | flops 268566528 | bytes 8716288 | tf_op jit(solution)/shard_map/dot_general | solution.py:103
  237.1 4.6 %all_to_all.61 = bf16[2,4096,64]{1,2,0:T(8,128)(2,1)S(1)} all-to-all(bf16[2,4096,64]{1,2,0:T(8,128)(2,1)S(1)} %broadcast_in_dim.35), channel_id=1, replica_groups=mesh['ep'=64,'tp'=2] {'tp'}, dimensions={0} | all-to-all | bytes 2097152 | tf_op jit(solution)/shard_map/all_to_all | solution.py:34
  241.7 16.9 %all-to-all-start.5 = ((bf16[64,4,1024]{2,1,0:T(4,128)(2,1)}), bf16[64,4,1024]{2,1,0:T(4,128)(2,1)S(1)}, u32[]{:S(2)}, u32[]{:S(2)}) async-start(bf16[64,4,1024]{2,1,0:T(4,128)(2,1)} %reshape.205), calls=%async_computation.5 | async-start | bytes 1048576 | tf_op jit(solution)/shard_map/all_to_all | solution.py:214
  259.0 0.5 all_to_all.47
  259.9 1.0 reshape.234
  260.9 11.4 %all-to-all-done.5 = bf16[64,4,1024]{2,1,0:T(4,128)(2,1)S(1)} async-done(((bf16[64,4,1024]{2,1,0:T(4,128)(2,1)}), bf16[64,4,1024]{2,1,0:T(4,128)(2,1)S(1)}, u32[]{:S(2)}, u32[]{:S(2)}) %all-to-all-start.5) | async-done | bytes 524320 | tf_op jit(solution)/shard_map/all_to_all | solution.py:214
  272.3 5.0 %all-to-all-start.8 = ((bf16[64,2,1024]{2,1,0:T(2,128)(2,1)}), bf16[64,2,1024]{2,1,0:T(2,128)(2,1)S(1)}, u32[]{:S(2)}, u32[]{:S(2)}) async-start(bf16[64,2,1024]{2,1,0:T(2,128)(2,1)} %reshape.234), calls=%async_computation.8 | async-start | bytes 524288 | tf_op jit(solution)/shard_map/all_to_all | solution.py:224
  277.4 0.9 gather_fusion
  278.6 0.7 multiply_reduce_fusion
  279.3 8.3 %all-to-all-done.8 = bf16[64,2,1024]{2,1,0:T(2,128)(2,1)S(1)} async-done(((bf16[64,2,1024]{2,1,0:T(2,128)(2,1)}), bf16[64,2,1024]{2,1,0:T(2,128)(2,1)S(1)}, u32[]{:S(2)}, u32[]{:S(2)}) %all-to-all-start.8) | async-done | bytes 262176 | tf_op jit(solution)/shard_map/all_to_all | solution.py:224
  288.0 3.9 %fusion.12 = bf16[64,1024]{1,0:T(8,128)(2,1)} fusion(bf16[64,2048]{0,1:T(8,128)(2,1)S(1)} %bitcast.78, bf16[2048,1024]{1,0:T(8,128)(2,1)} %param.49, f32[64,1024]{1,0:T(8,128)S(1)} %multiply_reduce_fusion, bf16[64,1024]{1,0:T(8,128)(2,1)S(1)} %get-tuple-element.28, f32[64]{0:T(128)S(1)} %fusion.73), kind=kOutput, calls=%fused_computation.21 | convolution fusion | flops 268763136 | bytes 4980992 | tf_op jit(solution)/shard_map/dot_general | solution.py:225
  (114 shorter events, 7.6 us)
Async XLA Ops:
  0.6 86.3 %copy-start = (bf16[1,512,2048]{2,1,0:T(8,128)(2,1)S(1)}, bf16[1,512,2048]{2,1,0:T(8,128)(2,1)}, u32[]{:S(2)}) copy-start(bf16[1,512,2048]{2,1,0:T(8,128)(2,1)} %param.46) | copy-start | bytes 6291460
  4.1 3.5 %copy-start.7 = (bf16[64,1024]{1,0:T(8,128)(2,1)S(1)}, bf16[64,1024]{1,0:T(8,128)(2,1)}, u32[]{:S(2)}) copy-start(bf16[64,1024]{1,0:T(8,128)(2,1)} %param.25) | copy-start | bytes 393220
  4.1 3.6 %copy-start.20 = (u32[128]{0:T(128)S(1)}, u32[128]{0:T(128)}, u32[]{:S(2)}) copy-start(u32[128]{0:T(128)} %constant.69) | copy-start | bytes 1540
  4.1 7.6 %copy-start.17 = (f32[2048]{0:T(1024)S(1)}, f32[2048]{0:T(1024)}, u32[]{:S(2)}) copy-start(f32[2048]{0:T(1024)} %param.28) | copy-start | bytes 24580
  4.1 9.5 %copy-start.19 = (f32[64]{0:T(128)S(1)}, f32[64]{0:T(128)}, u32[]{:S(2)}) copy-start(f32[64]{0:T(128)} %param.32) | copy-start | bytes 772
  4.1 10.5 %copy-start.8 = (f32[64,64,16]{1,2,0:T(8,128)S(1)}, f32[64,64,16]{1,2,0:T(8,128)}, u32[]{:S(2)}) copy-start(f32[64,64,16]{1,2,0:T(8,128)} %param.34) | copy-start | bytes 786436
  4.1 10.5 %copy-start.9 = (f32[64,64,16]{1,2,0:T(8,128)S(1)}, f32[64,64,16]{1,2,0:T(8,128)}, u32[]{:S(2)}) copy-start(f32[64,64,16]{1,2,0:T(8,128)} %param.33) | copy-start | bytes 786436
  14.7 4.0 %copy-start.5 = (f32[64,64,64]{0,2,1:T(8,128)S(1)}, f32[64,64,64]{0,2,1:T(8,128)}, u32[]{:S(2)}) copy-start(f32[64,64,64]{0,2,1:T(8,128)} %copy.204) | copy-start | bytes 3145732
  14.7 4.0 %copy-start.6 = (f32[64,64,64]{0,2,1:T(8,128)S(1)}, f32[64,64,64]{0,2,1:T(8,128)}, u32[]{:S(2)}) copy-start(f32[64,64,64]{0,2,1:T(8,128)} %copy.203) | copy-start | bytes 3145732
  18.7 2.5 copy-start.4
  18.7 2.5 copy-start.11
  21.2 1.9 copy-start.2
  21.2 1.4 copy-start.10
  22.6 0.7 copy-start.14
  30.1 7.3 %copy-start.18 = (f32[2048]{0:T(1024)S(1)}, f32[2048]{0:T(1024)}, u32[]{:S(2)}) copy-start(f32[2048]{0:T(1024)} %param.29) | copy-start | bytes 24580
  30.2 11.6 %copy-start.15 = (s32[64,2]{0,1:T(2,128)S(1)}, s32[64,2]{0,1:T(2,128)}, u32[]{:S(2)}) copy-start(s32[64,2]{0,1:T(2,128)} %param.43) | copy-start | bytes 1540
  38.3 5.0 %all-to-all-start.2 = ((bf16[2,64,1024]{2,1,0:T(8,128)(2,1)}), bf16[2,64,1024]{2,1,0:T(8,128)(2,1)S(1)}, u32[]{:S(2)}, u32[]{:S(2)}) async-start(bf16[2,64,1024]{2,1,0:T(8,128)(2,1)} %broadcast_in_dim.33), calls=%async_computation.2 | async-start | bytes 524288 | tf_op jit(solution)/shard_map/all_to_all | solution.py:34
  46.5 12.8 %copy-start.16 = (bf16[2048,4]{0,1:T(4,128)(2,1)S(1)}, bf16[2048,4]{0,1:T(4,128)(2,1)}, u32[]{:S(2)}) copy-start(bf16[2048,4]{0,1:T(4,128)(2,1)} %param.40) | copy-start | bytes 49156
  46.5 14.1 %dynamic-slice-start = ((f32[2048]{0:T(1024)}, s32[]{:T(128)}), f32[1024]{0:T(1024)S(1)}, s32[]{:S(2)}) async-start(f32[2048]{0:T(1024)} %param.42, s32[]{:T(128)} %select_n.31), calls=%async_computation.9 | async-start | bytes 8704 | tf_op jit(solution)/shard_map/dynamic_slice | solution.py:140
  47.7 30.7 %all-to-all-start.3 = ((bf16[64,4,2048]{2,1,0:T(4,128)(2,1)}), bf16[64,4,2048]{2,1,0:T(4,128)(2,1)S(1)}, u32[]{:S(2)}, u32[]{:S(2)}) async-start(bf16[64,4,2048]{2,1,0:T(4,128)(2,1)} %reshape.203), calls=%async_computation.3 | async-start | bytes 2097152 | tf_op jit(solution)/shard_map/all_to_all | solution.py:203
  79.1 11.1 %all-to-all-start.1 = ((f32[2,1,4416]{2,1,0:T(1,128)}), f32[2,1,4416]{2,1,0:T(1,128)S(1)}, u32[]{:S(2)}, u32[]{:S(2)}) async-start(f32[2,1,4416]{2,1,0:T(1,128)} %broadcast_in_dim.24), calls=%async_computation.1 | async-start | bytes 71680 | tf_op jit(solution)/shard_map/all_to_all | solution.py:34
  101.1 124.0 %all-to-all-start.6 = ((bf16[64,64,1024]{2,1,0:T(8,128)(2,1)}), bf16[64,64,1024]{2,1,0:T(8,128)(2,1)}, u32[]{:S(2)}, u32[]{:S(2)}) async-start(bf16[64,64,1024]{2,1,0:T(8,128)(2,1)} %stack.11), calls=%async_computation.6 | async-start | bytes 16777216 | tf_op jit(solution)/shard_map/all_to_all | solution.py:12
  107.0 3.9 %copy-start.3 = (f32[64,64,64]{0,2,1:T(8,128)S(1)}, f32[64,64,64]{0,2,1:T(8,128)}, u32[]{:S(2)}) copy-start(f32[64,64,64]{0,2,1:T(8,128)} %copy-done.2) | copy-start | bytes 3145732
  114.7 110.3 %copy-start.12 = (bf16[1024,32]{0,1:T(8,128)(2,1)S(1)}, bf16[1024,32]{0,1:T(8,128)(2,1)}, u32[]{:S(2)}) copy-start(bf16[1024,32]{0,1:T(8,128)(2,1)} %param.48) | copy-start | bytes 196612
  225.0 6.0 %copy-start.13 = (bf16[1024,32]{0,1:T(8,128)(2,1)S(1)}, bf16[1024,32]{0,1:T(8,128)(2,1)}, u32[]{:S(2)}) copy-start(bf16[1024,32]{0,1:T(8,128)(2,1)} %param.47) | copy-start | bytes 196612
  241.7 30.6 %all-to-all-start.5 = ((bf16[64,4,1024]{2,1,0:T(4,128)(2,1)}), bf16[64,4,1024]{2,1,0:T(4,128)(2,1)S(1)}, u32[]{:S(2)}, u32[]{:S(2)}) async-start(bf16[64,4,1024]{2,1,0:T(4,128)(2,1)} %reshape.205), calls=%async_computation.5 | async-start | bytes 1048576 | tf_op jit(solution)/shard_map/all_to_all | solution.py:214
  272.3 15.3 %all-to-all-start.8 = ((bf16[64,2,1024]{2,1,0:T(2,128)(2,1)}), bf16[64,2,1024]{2,1,0:T(2,128)(2,1)S(1)}, u32[]{:S(2)}, u32[]{:S(2)}) async-start(bf16[64,2,1024]{2,1,0:T(2,128)(2,1)} %reshape.234), calls=%async_computation.8 | async-start | bytes 524288 | tf_op jit(solution)/shard_map/all_to_all | solution.py:224
  288.0 3.9 %copy-start.1 = (bf16[1,512,2048]{2,1,0:T(8,128)(2,1)S(1)}, bf16[1,512,2048]{2,1,0:T(8,128)(2,1)}, u32[]{:S(2)}) copy-start(bf16[1,512,2048]{2,1,0:T(8,128)(2,1)} %param.46) | copy-start | bytes 6291460
